TPU v7x, 32 devices: a whole 2x2x4 slice. The times are simulated.
32 devices in a mesh: sp: 8 (over z, y), tp: 4 (over x, core).
Axes of the slice: x: 2, y: 2, z: 4, core: 2. Of those that a mesh axis runs over, the one named last changes fastest.
Arguments:
- tokens: bfloat16 [4, 1024, 2048], P(None, 'sp'), may hold values from -6 to 6
- next_tokens: bfloat16 [4, 2048], replicated, may hold values from -6 to 6
- w_query: bfloat16 [2048, 2048], P(None, 'tp'), may hold values from -0.125 to 0.125
- w_key: bfloat16 [2048, 2048], P(None, 'tp'), may hold values from -0.125 to 0.125
- w_value: bfloat16 [2048, 2048], P(None, 'tp'), may hold values from -0.125 to 0.125
- w_in_gate: bfloat16 [2048, 8], replicated, may hold values from -0.125 to 0.125
- w_forget_gate: bfloat16 [2048, 8], replicated, may hold values from -0.125 to 0.125
- forget_bias: float32 [8], replicated, may hold values from 3 to 14
- extra_decay: float32 [8, 4, 1024], P('tp', None, 'sp'), may hold values from -0.5509766 to 0
- w_out: bfloat16 [2048, 2048], P('tp'), may hold values from -0.125 to 0.125
Outputs:
- memory: bfloat16 [8, 1024, 256], P('tp', 'sp')
- normalizer: float32 [8, 1024], P('tp', 'sp')
- stabilizer: float32 [4, 8], P(None, 'tp')
- read: bfloat16 [4, 2048], replicated
All inputs are finite; a program needn't handle non-finite values.
Results may differ from a plain program's by a relative error of at most 0.024.
Values may be sent and summed in bfloat16 or wider, within the bound.
A program may use at most 64 MiB of HBM per device.

v0:
```python
import jax
import jax.numpy as jnp
from jax import lax
from jax.sharding import PartitionSpec as P

HD = 256


def per_device(
    tokens,
    next_tokens,
    w_query,
    w_key,
    w_value,
    w_in_gate,
    w_forget_gate,
    forget_bias,
    extra_decay,
    w_out,
):
    scale = HD ** (-0.5)
    seq_count = tokens.shape[0]
    span = tokens.shape[1]
    heads_here = w_key.shape[1] // HD
    sp_size = lax.axis_size("sp")
    sp_index = lax.axis_index("sp")
    head_start = lax.axis_index("tp") * heads_here
    gate_in = lax.dynamic_slice_in_dim(w_in_gate, head_start, heads_here, 1)
    gate_forget = lax.dynamic_slice_in_dim(w_forget_gate, head_start, heads_here, 1)
    bias_here = lax.dynamic_slice_in_dim(forget_bias, head_start, heads_here, 0)
    flat = tokens.reshape(seq_count * span, tokens.shape[2])
    keys = jnp.dot(flat, w_key, preferred_element_type=jnp.float32).astype(jnp.bfloat16)
    values = jnp.dot(flat, w_value, preferred_element_type=jnp.float32).astype(jnp.bfloat16)
    log_in = jnp.dot(flat, gate_in, preferred_element_type=jnp.float32).reshape(
        seq_count, span, heads_here
    )
    log_forget = jax.nn.log_sigmoid(
        jnp.dot(flat, gate_forget, preferred_element_type=jnp.float32) + bias_here
    ).reshape(seq_count, span, heads_here) + jnp.transpose(extra_decay, (1, 2, 0))
    prefix = jnp.cumsum(log_forget, axis=1)
    block_total = prefix[:, -1]
    local_score = block_total[:, None, :] - prefix + log_in
    block_peak = jnp.max(local_score, axis=1)
    totals, peaks = (
        lax.all_gather(block_total[None], "sp", axis=0, tiled=True),
        lax.all_gather(block_peak[None], "sp", axis=0, tiled=True),
    )
    later = jnp.flip(jnp.cumsum(jnp.flip(totals, 0), axis=0), 0) - totals
    prompt_total = jnp.sum(totals, axis=0)
    stabilizer = jnp.maximum(prompt_total, jnp.max(later + peaks, axis=0))
    pick_block = (jnp.arange(sp_size) == sp_index).astype(jnp.float32)
    later_here = jnp.sum(pick_block[:, None, None] * later, axis=0)
    weight = jnp.exp(later_here[:, None, :] + local_score - stabilizer[:, None, :]) * scale
    key_heads = keys.reshape(seq_count, span, heads_here, HD)
    value_heads = values.reshape(seq_count, span, heads_here, HD)
    weighted = (key_heads.astype(jnp.float32) * weight[:, :, :, None]).astype(jnp.bfloat16)
    block_memory = jnp.einsum(
        "sthd,sthe->hsde", weighted, value_heads, preferred_element_type=jnp.float32
    )
    block_norm = jnp.transpose(jnp.sum(weighted.astype(jnp.float32), axis=1), (1, 0, 2))
    memory_term = block_memory.reshape(heads_here, seq_count * HD, HD)
    norm_term = block_norm.reshape(heads_here, seq_count * HD)
    memory_rows, norm_rows = (
        lax.psum_scatter(memory_term, "sp", scatter_dimension=1, tiled=True),
        lax.psum_scatter(norm_term, "sp", scatter_dimension=1, tiled=True),
    )
    query = (
        jnp.dot(next_tokens, w_query, preferred_element_type=jnp.float32)
        .astype(jnp.bfloat16)
        .astype(jnp.float32)
        .reshape(seq_count, heads_here, HD)
    )
    new_key = (
        jnp.dot(next_tokens, w_key, preferred_element_type=jnp.float32)
        .astype(jnp.bfloat16)
        .astype(jnp.float32)
        .reshape(seq_count, heads_here, HD)
        * scale
    )
    new_value = (
        jnp.dot(next_tokens, w_value, preferred_element_type=jnp.float32)
        .astype(jnp.bfloat16)
        .astype(jnp.float32)
        .reshape(seq_count, heads_here, HD)
    )
    new_in = jnp.dot(next_tokens, gate_in, preferred_element_type=jnp.float32)
    new_forget = jax.nn.log_sigmoid(
        jnp.dot(next_tokens, gate_forget, preferred_element_type=jnp.float32) + bias_here
    )
    numer_slots = jnp.einsum("shd,hsde->she", query, block_memory, precision=lax.Precision.HIGHEST)
    denom_slots = jnp.einsum("shd,hsd->sh", query, block_norm, precision=lax.Precision.HIGHEST)
    query_state, query_norm = lax.psum((numer_slots, denom_slots), "sp")
    top = jnp.maximum(new_forget + stabilizer, new_in)
    keep = jnp.exp(new_forget + stabilizer - top)
    take = jnp.exp(new_in - top)
    qk = jnp.sum(query * new_key, axis=-1)
    numer = keep[:, :, None] * query_state + (take * qk)[:, :, None] * new_value
    denom = keep * query_norm + take * qk
    head_out = (numer / jnp.maximum(jnp.abs(denom), 1.0)[:, :, None]).astype(jnp.bfloat16)
    partial_value = (
        jnp.dot(
            head_out.reshape(seq_count, heads_here * HD), w_out, preferred_element_type=jnp.float32
        )
        .astype(jnp.bfloat16)
        .astype(jnp.float32)
    )
    read = lax.psum(partial_value.astype(jnp.bfloat16), "tp")
    return (memory_rows.astype(jnp.bfloat16), norm_rows, stabilizer, read)


def solution(mesh):
    placed = (
        P(None, "sp", None),
        P(),
        P(None, "tp"),
        P(None, "tp"),
        P(None, "tp"),
        P(),
        P(),
        P(),
        P("tp", None, "sp"),
        P("tp", None),
    )
    return jax.shard_map(
        per_device,
        mesh=mesh,
        in_specs=placed,
        out_specs=(P("tp", "sp", None), P("tp", "sp"), P(None, "tp"), P()),
        check_vma=False,
    )
```

profile of v0, /device:TPU:0, one launch (start us, length us, event | category | flops | bytes accessed | tf_op | source)
XLA Modules:
  0.0 210.3 jit_solution(8536744384994718266)
XLA Ops:
  8.8 1.4 fusion.16
  10.7 27.9 %all-gather = f32[32,1,2]{2,1,0:T(1,128)S(1)} all-gather(f32[4,1,2]{2,1,0:T(1,128)S(1)} %slice.4), channel_id=2, replica_groups=mesh['sp'=8,'tp'=4] {'sp'}, dimensions={0}, use_global_device_ids=true | all-gather | bytes 288 | tf_op jit(solution)/shard_map/all_gather | solution.py:45
  38.8 2.8 %fusion.2 = f32[512,512]{1,0:T(8,128)S(1)} fusion(bf16[512,2048]{1,0:T(8,128)(2,1)S(1)} %bitcast.53, bf16[2048,512]{1,0:T(8,128)(2,1)} %param.13), kind=kOutput, calls=%fused_computation.5 | convolution fusion | flops 1074266112 | bytes 5242880 | tf_op jit(solution)/shard_map/dot_general | solution.py:32
  41.6 1.6 reshape.82
  43.3 1.5 copy.50
  46.4 1.0 fusion.13
  47.5 19.0 %all-gather.2 = f32[8,4,2]{1,2,0:T(2,128)S(1)} all-gather(f32[1,4,2]{1,2,0:T(2,128)S(1)} %bitcast.68), channel_id=3, replica_groups=mesh['sp'=8,'tp'=4] {'sp'}, dimensions={0}, use_global_device_ids=true | all-gather | bytes 288 | tf_op jit(solution)/shard_map/all_gather | solution.py:46
  66.8 1.7 exponential_multiply_fusion
  68.5 1.1 copy.49
  69.9 1.0 copy.68
  71.0 3.6 %convolution_convert_fusion.1 = bf16[512,512]{1,0:T(8,128)(2,1)} fusion(bf16[512,2048]{1,0:T(8,128)(2,1)S(1)} %bitcast.56, bf16[2048,512]{1,0:T(8,128)(2,1)} %param.14), kind=kOutput, calls=%fused_computation.3 | convolution fusion | flops 1074003968 | bytes 4718592 | tf_op jit(solution)/shard_map/dot_general | solution.py:33
  74.6 2.0 reshape.75
  76.6 2.8 %fusion.11 = f32[2,4,256,256]{3,2,1,0:T(8,128)} fusion(bf16[4,128,2,256]{3,2,1,0:T(2,128)(2,1)} %reshape.75, f32[4,128,2,256]{1,3,0,2:T(8,128)S(1)} %copy.50, f32[4,128,2]{1,0,2:T(4,128)S(1)} %copy.49), kind=kOutput, calls=%fused_computation.23 | convolution fusion | flops 134742016 | bytes 3674112 | tf_op jit(solution)/shard_map/sthd,sthe->hsde/dot_general | solution.py:57
  79.5 2.0 convolution_convert_fusion.5
  81.5 2.4 %fusion = f32[4,2,1,256]{3,2,1,0:T(1,128)S(1)} fusion(bf16[4,2,256,1]{2,3,1,0:T(2,128)(2,1)S(1)} %reshape.95, f32[2,4,256,256]{3,2,1,0:T(8,128)} %fusion.11), kind=kOutput, calls=%fused_computation.1 | convolution fusion | flops 6291456 | bytes 2109440 | tf_op jit(solution)/shard_map/shd,hsde->she/dot_general | solution.py:90
  84.0 17.7 %all-reduce = (f32[4,2]{0,1:T(2,128)S(1)}, f32[4,2,256]{2,1,0:T(2,128)S(1)}) all-reduce(f32[4,2]{0,1:T(2,128)S(1)} %multiply_reduce_fusion, f32[4,2,256]{2,1,0:T(2,128)S(1)} %bitcast.66), channel_id=1, replica_groups=mesh['sp'=8,'tp'=4] {'sp'}, use_global_device_ids=true, to_apply=%region_11.12 | all-reduce | flops 2056 | bytes 16448 | tf_op jit(solution)/shard_map/psum | solution.py:92
  101.7 2.0 fusion.6
  105.0 2.0 fusion.3
  107.3 2.0 convolution_convert_fusion
  109.3 10.7 %psum.23 = bf16[4,2048]{1,0:T(4,128)(2,1)} all-reduce(bf16[4,2048]{1,0:T(4,128)(2,1)S(1)} %convolution_convert_fusion), channel_id=1, replica_groups=mesh['sp'=8,'tp'=4] {'tp'}, use_global_device_ids=true, to_apply=%region_12.13 | all-reduce | flops 8192 | bytes 32768 | tf_op jit(solution)/shard_map/psum | solution.py:107
  120.0 11.0 %reduce-scatter.7.cloned.1.call-done = f32[128,2]{1,0:T(8,128)} async-done(((f32[1024,2]{1,0:T(8,128)}), f32[128,2]{1,0:T(8,128)}) %reduce-scatter.7.cloned.1.call-update) | async-done | bytes 1040
  131.0 1.5 copy.67
  132.5 69.4 %reduce-scatter.5.cloned.1.call-done = f32[2,128,256]{2,1,0:T(8,128)} async-done(((f32[2,1024,256]{2,1,0:T(8,128)}), f32[2,128,256]{2,1,0:T(8,128)}) %reduce-scatter.5.cloned.1.call-update) | async-done | bytes 262160 | tf_op jit(solution)/shard_map/reduce_scatter | solution.py:64
  201.9 1.6 convert_element_type.58
  (51 shorter events, 6.4 us)
Async XLA Ops:
  7.2 1.6 copy-start
  7.2 3.1 %copy-start.2 = (f32[2,4,128]{2,1,0:T(4,128)S(1)}, f32[2,4,128]{2,1,0:T(4,128)}, u32[]{:S(2)}) copy-start(f32[2,4,128]{2,1,0:T(4,128)} %param.18) | copy-start | bytes 12292
  7.2 123.8 %reduce-scatter.7.cloned.1.call-start = ((), (), s32[]{:S(2)}) async-start(), calls=%async_computation.3 | async-start | bytes 589824
  41.6 3.3 %copy-start.4 = (bf16[2048,8]{0,1:T(8,128)(2,1)S(1)}, bf16[2048,8]{0,1:T(8,128)(2,1)}, u32[]{:S(2)}) copy-start(bf16[2048,8]{0,1:T(8,128)(2,1)} %param.15) | copy-start | bytes 98308
  66.6 37.5 %copy-start.3 = (f32[4,2]{0,1:T(2,128)}, f32[4,2]{0,1:T(2,128)S(1)}, u32[]{:S(2)}) copy-start(f32[4,2]{0,1:T(2,128)S(1)} %max.30) | copy-start | bytes 100
  71.0 130.9 %reduce-scatter.5.cloned.1.call-start = ((), (), s32[]{:S(2)}) async-start(), calls=%async_computation.2 | async-start | bytes 2359296 | tf_op jit(solution)/shard_map/reduce_scatter | solution.py:64
  76.6 2.9 %copy-start.1 = (bf16[4,2048]{1,0:T(4,128)(2,1)S(1)}, bf16[4,2048]{1,0:T(4,128)(2,1)}, u32[]{:S(2)}) copy-start(bf16[4,2048]{1,0:T(4,128)(2,1)} %param.11) | copy-start | bytes 49156
Sparse Core Ops, SparseCore 0:
  71.1 59.8 reduce-scatter.6
  134.5 67.3 reduce-scatter.4
where the time goes:
time: 211 us; the launch traced here: 210 us
  waiting for transfers between devices  80.4 us (38%)
  blocking collectives  75.4 us (36%)
  matrix products  22.7 us (11%)
  between operations  14.2 us (7%)
  local copies, waits for them, and re-layouts  12.2 us (6%)
  other arithmetic  5.39 us (3%)
    reduce_scatter x1, waiting for transfers between devices, per_device(): lax.psum_scatter(memory_term, 'sp', scatter_dimension=1, tiled=True)  69.4 us
    all_gather x1, blocking collectives, per_device(): lax.all_gather(block_total[None], 'sp', axis=0, tiled=True)  27.9 us
    all_gather x1, blocking collectives, per_device(): lax.all_gather(block_peak[None], 'sp', axis=0, tiled=True)  19 us
    psum x1, blocking collectives, per_device(): query_state, query_norm = lax.psum((numer_slots, denom_slots), 'sp')  17.7 us
    unnamed x3, waiting for transfers between devices  11 us
    psum x1, blocking collectives, per_device(): read = lax.psum(partial_value.astype(jnp.bfloat16), 'tp')  10.7 us
  transfers between devices with their start and end apart: 2, of which 2 were waited for; matrix products, arithmetic and copies ran while one was open for 10% of the time, Pallas kernels for 0%

commit v1 on v0

--- a/solution.py
+++ b/solution.py
@@ -4,6 +4,11 @@
 from jax.sharding import PartitionSpec as P
 
 HD = 256
+
+
+def gather_over(x, name, dim):
+    stack = jnp.stack([x] * lax.axis_size(name))
+    return jnp.concatenate(lax.all_to_all(stack, name, 0, 0), axis=dim)
 
 
 def per_device(
@@ -43,7 +48,7 @@
     block_peak = jnp.max(local_score, axis=1)
     totals, peaks = (
         lax.all_gather(block_total[None], "sp", axis=0, tiled=True),
-        lax.all_gather(block_peak[None], "sp", axis=0, tiled=True),
+        gather_over(block_peak[None], "sp", 0),
     )
     later = jnp.flip(jnp.cumsum(jnp.flip(totals, 0), axis=0), 0) - totals
     prompt_total = jnp.sum(totals, axis=0)

time: 211 us -> 204 us (0.967)
  blocking collectives: 75.4 us -> 57.8 us
  starting transfers between devices: 0.08 us -> 7.39 us
  waiting for transfers between devices: 80.4 us -> 85.4 us
    all_gather x1 -> x0, blocking collectives: 19 us -> none  [per_device(): lax.all_gather(block_peak[None], 'sp', axis=0, tiled=True)]
    all_to_all x0 -> x1, starting transfers between devices: none -> 7.31 us  [gather_over(): return jnp.concatenate(lax.all_to_all(stack, name, 0, 0), axis=dim)]
    unnamed x3, waiting for transfers between devices: 11 us -> 16 us
    psum x1, blocking collectives: 17.7 us -> 20.3 us  [per_device(): query_state, query_norm = lax.psum((numer_slots, denom_slots), 'sp')]
  transfers between devices with their start and end apart: 2 -> 3, of which waited for: 2 -> 2; matrix products, arithmetic and copies ran while one was open for 10% -> 13% of each run, Pallas kernels for 0% -> 0%
where the time goes in v1:
time: 204 us; the launch traced here: 203 us
  waiting for transfers between devices  85.4 us (42%)
  blocking collectives  57.8 us (28%)
  matrix products  21.4 us (10%)
  between operations  14.3 us (7%)
  local copies, waits for them, and re-layouts  12.4 us (6%)
  starting transfers between devices  7.39 us (4%)
  other arithmetic  4.42 us (2%)
    reduce_scatter x1, waiting for transfers between devices, per_device(): lax.psum_scatter(memory_term, 'sp', scatter_dimension=1, tiled=True)  69.4 us
    all_gather x1, blocking collectives, per_device(): lax.all_gather(block_total[None], 'sp', axis=0, tiled=True)  26.6 us
    psum x1, blocking collectives, per_device(): query_state, query_norm = lax.psum((numer_slots, denom_slots), 'sp')  20.3 us
    unnamed x3, waiting for transfers between devices  16 us
    psum x1, blocking collectives, per_device(): read = lax.psum(partial_value.astype(jnp.bfloat16), 'tp')  10.9 us
    all_to_all x1, starting transfers between devices, gather_over(): return jnp.concatenate(lax.all_to_all(stack, name, 0, 0), axis=dim)  7.31 us
    convert_element_type x2, local copies, waits for them, and re-layouts, per_device(): key_heads.astype(jnp.float32) * weight[:, :, :, None]  4.36 us
  transfers between devices with their start and end apart: 3, of which 2 were waited for; matrix products, arithmetic and copies ran while one was open for 13% of the time, Pallas kernels for 0%

profile of v1, /device:TPU:0, one launch (start us, length us, event | category | flops | bytes accessed | tf_op | source)
XLA Modules:
  0.0 203.2 jit_solution(12673208738392232505)
XLA Ops:
  8.8 1.4 fusion.16
  12.3 7.3 %all-to-all-start = ((f32[8,1,4,2]{2,3,1,0:T(2,128)}), f32[8,1,4,2]{2,3,1,0:T(2,128)S(1)}, u32[]{:S(2)}, u32[]{:S(2)}) async-start(f32[8,1,4,2]{2,3,1,0:T(2,128)} %stack.3), calls=%async_computation | async-start | bytes 16384 | tf_op jit(solution)/shard_map/all_to_all | solution.py:11
  19.6 26.6 %all-gather = f32[32,1,2]{2,1,0:T(1,128)S(1)} all-gather(f32[4,1,2]{2,1,0:T(1,128)S(1)} %slice.4), channel_id=2, replica_groups=mesh['sp'=8,'tp'=4] {'sp'}, dimensions={0}, use_global_device_ids=true | all-gather | bytes 288 | tf_op jit(solution)/shard_map/all_gather | solution.py:50
  46.2 3.0 %convolution_convert_fusion.1 = bf16[512,512]{1,0:T(8,128)(2,1)S(1)} fusion(bf16[512,2048]{1,0:T(8,128)(2,1)S(1)} %bitcast.56, bf16[2048,512]{1,0:T(8,128)(2,1)} %param.14), kind=kOutput, calls=%fused_computation.3 | convolution fusion | flops 1074003968 | bytes 4718592 | tf_op jit(solution)/shard_map/dot_general | solution.py:38
  49.3 2.3 %fusion.2 = f32[512,512]{1,0:T(8,128)} fusion(bf16[512,2048]{1,0:T(8,128)(2,1)S(1)} %bitcast.53, bf16[2048,512]{1,0:T(8,128)(2,1)S(1)} %copy-done.2), kind=kOutput, calls=%fused_computation.5 | convolution fusion | flops 1074266112 | bytes 5242880 | tf_op jit(solution)/shard_map/dot_general | solution.py:37
  51.7 0.9 reshape.81
  52.6 2.9 %reshape.88 = f32[4,128,2,256]{3,2,1,0:T(2,128)} reshape(f32[512,512]{1,0:T(8,128)} %fusion.2) | data formatting | bytes 2097152 | tf_op jit(solution)/shard_map/convert_element_type | solution.py:61
  55.5 1.5 copy.51
  57.4 1.7 exponential_multiply_fusion
  59.1 1.1 copy.50
  60.5 1.1 copy.71
  61.7 2.8 %fusion.11 = f32[2,4,256,256]{3,2,1,0:T(8,128)} fusion(bf16[4,128,2,256]{3,2,1,0:T(2,128)(2,1)} %reshape.81, f32[4,128,2,256]{1,3,0,2:T(8,128)S(1)} %copy.51, f32[4,128,2]{1,0,2:T(4,128)S(1)} %copy.50), kind=kOutput, calls=%fused_computation.23 | convolution fusion | flops 134742016 | bytes 3674112 | tf_op jit(solution)/shard_map/sthd,sthe->hsde/dot_general | solution.py:62
  64.5 2.0 convolution_convert_fusion.5
  66.5 2.0 fusion.6
  68.7 2.0 fusion.3
  70.8 2.4 %fusion = f32[4,2,1,256]{3,2,1,0:T(1,128)S(1)} fusion(bf16[4,2,256,1]{2,3,1,0:T(2,128)(2,1)S(1)} %reshape.97, f32[2,4,256,256]{3,2,1,0:T(8,128)} %fusion.11), kind=kOutput, calls=%fused_computation.1 | convolution fusion | flops 6291456 | bytes 2109440 | tf_op jit(solution)/shard_map/shd,hsde->she/dot_general | solution.py:95
  73.3 20.3 %all-reduce = (f32[4,2]{0,1:T(2,128)S(1)}, f32[4,2,256]{2,1,0:T(2,128)S(1)}) all-reduce(f32[4,2]{0,1:T(2,128)S(1)} %multiply_reduce_fusion, f32[4,2,256]{2,1,0:T(2,128)S(1)} %bitcast.67), channel_id=1, replica_groups=mesh['sp'=8,'tp'=4] {'sp'}, use_global_device_ids=true, to_apply=%region_11.12 | all-reduce | flops 2056 | bytes 16448 | tf_op jit(solution)/shard_map/psum | solution.py:97
  93.7 0.9 abs_maximum_fusion
  95.0 2.0 convolution_convert_fusion
  97.0 10.9 %psum.23 = bf16[4,2048]{1,0:T(4,128)(2,1)} all-reduce(bf16[4,2048]{1,0:T(4,128)(2,1)S(1)} %convolution_convert_fusion), channel_id=1, replica_groups=mesh['sp'=8,'tp'=4] {'tp'}, use_global_device_ids=true, to_apply=%region_12.13 | all-reduce | flops 8192 | bytes 32768 | tf_op jit(solution)/shard_map/psum | solution.py:112
  107.8 16.0 %reduce-scatter.7.cloned.1.call-done = f32[128,2]{1,0:T(8,128)} async-done(((f32[1024,2]{1,0:T(8,128)}), f32[128,2]{1,0:T(8,128)}) %reduce-scatter.7.cloned.1.call-update) | async-done | bytes 1040
  123.8 1.5 copy.70
  125.3 69.4 %reduce-scatter.5.cloned.1.call-done = f32[2,128,256]{2,1,0:T(8,128)} async-done(((f32[2,1024,256]{2,1,0:T(8,128)}), f32[2,128,256]{2,1,0:T(8,128)}) %reduce-scatter.5.cloned.1.call-update) | async-done | bytes 262160 | tf_op jit(solution)/shard_map/reduce_scatter | solution.py:69
  194.7 1.6 convert_element_type.58
  (57 shorter events, 5.5 us)
Async XLA Ops:
  7.2 1.6 copy-start
  7.2 3.1 %copy-start.4 = (f32[2,4,128]{2,1,0:T(4,128)S(1)}, f32[2,4,128]{2,1,0:T(4,128)}, u32[]{:S(2)}) copy-start(f32[2,4,128]{2,1,0:T(4,128)} %param.18) | copy-start | bytes 12292
  7.2 3.5 %copy-start.6 = (bf16[2048,8]{0,1:T(8,128)(2,1)S(1)}, bf16[2048,8]{0,1:T(8,128)(2,1)}, u32[]{:S(2)}) copy-start(bf16[2048,8]{0,1:T(8,128)(2,1)} %param.15) | copy-start | bytes 98308
  11.5 37.7 %copy-start.1 = (f32[512,2]{1,0:T(8,128)}, f32[512,2]{1,0:T(8,128)S(1)}, u32[]{:S(2)}) copy-start(f32[512,2]{1,0:T(8,128)S(1)} %copy.66) | copy-start | bytes 12292
  12.3 44.8 %all-to-all-start = ((f32[8,1,4,2]{2,3,1,0:T(2,128)}), f32[8,1,4,2]{2,3,1,0:T(2,128)S(1)}, u32[]{:S(2)}, u32[]{:S(2)}) async-start(f32[8,1,4,2]{2,3,1,0:T(2,128)} %stack.3), calls=%async_computation | async-start | bytes 16384 | tf_op jit(solution)/shard_map/all_to_all | solution.py:11
  19.6 104.2 %reduce-scatter.7.cloned.1.call-start = ((), (), s32[]{:S(2)}) async-start(), calls=%async_computation.4 | async-start | bytes 589824
  46.2 3.0 %copy-start.2 = (bf16[2048,512]{1,0:T(8,128)(2,1)S(1)}, bf16[2048,512]{1,0:T(8,128)(2,1)}, u32[]{:S(2)}) copy-start(bf16[2048,512]{1,0:T(8,128)(2,1)} %param.13) | copy-start | bytes 6291460
  57.2 36.5 %copy-start.5 = (f32[4,2]{0,1:T(2,128)}, f32[4,2]{0,1:T(2,128)S(1)}, u32[]{:S(2)}) copy-start(f32[4,2]{0,1:T(2,128)S(1)} %max.30) | copy-start | bytes 100
  61.6 2.9 %copy-start.3 = (bf16[4,2048]{1,0:T(4,128)(2,1)S(1)}, bf16[4,2048]{1,0:T(4,128)(2,1)}, u32[]{:S(2)}) copy-start(bf16[4,2048]{1,0:T(4,128)(2,1)} %param.11) | copy-start | bytes 49156
  61.6 133.1 %reduce-scatter.5.cloned.1.call-start = ((), (), s32[]{:S(2)}) async-start(), calls=%async_computation.3 | async-start | bytes 2359296 | tf_op jit(solution)/shard_map/reduce_scatter | solution.py:69
Sparse Core Ops, SparseCore 0:
  61.7 62.0 reduce-scatter.6
  127.3 67.3 reduce-scatter.4
